TPU v7x, 32 devices: a whole 2x2x4 slice. The times are simulated.
32 devices in a mesh: sp: 8 (over z, y), tp: 4 (over x, core).
Axes of the slice: x: 2, y: 2, z: 4, core: 2. Of those that a mesh axis runs over, the one named last changes fastest.
Arguments:
- mix_input: bfloat16 [2048, 1024], P('sp', 'tp'), may hold values from -6 to 6
- stream: bfloat16 [2048, 2048], P(('sp', 'tp')), may hold values from -48 to 48
- doc_ids: int32 [2048], P('sp'), may hold values from 0 to 3, never falling along the last dimension, each value on 1 to 1024 neighbouring positions
- log_dt: float32 [64], P('tp'), may hold values from -12 to -2
- decay_rate: float32 [64, 64], P('tp'), may hold values from 0.5 to 1
- frequency: float32 [64, 64], P('tp'), may hold values from 0 to 64
- input_real: float32 [2, 64, 64, 16], P(None, 'tp'), may hold values from -400 to 400
- input_imag: float32 [2, 64, 64, 16], P(None, 'tp'), may hold values from -400 to 400
- output_real: float32 [2, 64, 16, 64], P(None, 'tp'), may hold values from -0.75 to 0.75
- output_imag: float32 [2, 64, 16, 64], P(None, 'tp'), may hold values from -0.75 to 0.75
- skip_gain: float32 [1024], P('tp'), may hold values from -4 to 4
- log_keep: float32 [64, 2048], P('tp', 'sp'), may hold values from -2 to 0
- proj_weight: bfloat16 [1024, 2048], P('tp'), may hold values from -0.1875 to 0.1875
- norm_gain: float32 [2048], replicated, may hold values from 0.1 to 1.9
- gate_weight: bfloat16 [2048, 5632], P('sp', 'tp'), may hold values from -0.125 to 0.125
- up_weight: bfloat16 [2048, 5632], P('sp', 'tp'), may hold values from -0.125 to 0.125
- down_weight: bfloat16 [5632, 2048], P('tp', 'sp'), may hold values from -0.078125 to 0.078125
Outputs:
- layer_out: bfloat16 [2048, 2048], P(('sp', 'tp'))
Inputs may be any that keep to these rules, and one draw needn't show every extreme that they name: `doc_ids`: document numbers never fall along the positions; a document covers at most half of the positions.
All inputs are finite; a program needn't handle non-finite values.
Results may differ from a plain program's by a relative error of at most 0.009.
Values may be sent and summed in bfloat16 or wider, within the bound.
A program may use at most 128 MiB of HBM per device.

v0:
```python
import jax
import jax.numpy as jnp
from jax import lax
from jax.sharding import PartitionSpec as P

GROUP = 16


HIGHEST = lax.Precision.HIGHEST


def prefix(array, axis, combine, identity, reverse):
    devices, here = (lax.axis_size(axis), lax.axis_index(axis))
    everything = jax.tree.map(lambda part: lax.all_gather(part, axis), array)
    start = jax.tree.map(
        lambda part, zero: jnp.broadcast_to(jnp.asarray(zero, part.dtype), part.shape),
        array,
        identity,
    )

    def hop(k, before):
        at = devices - 1 - k if reverse else k
        reached = at > here if reverse else at < here
        new = combine(before, jax.tree.map(lambda part: part[at], everything))
        return jax.tree.map(lambda a, b: jnp.where(reached, a, b), new, before)

    return lax.fori_loop(0, devices, hop, start)


def discretize(log_dt, decay_rate, frequency):
    step_size = jnp.exp(log_dt)[:, None]
    magnitude = jnp.exp(-step_size * decay_rate)
    angle_step = step_size * frequency
    state_real = magnitude * jnp.cos(angle_step)
    state_imag = magnitude * jnp.sin(angle_step)
    denominator = decay_rate * decay_rate + frequency * frequency
    shifted = state_real - 1.0
    zoh_real = (-shifted * decay_rate + state_imag * frequency) / denominator
    holdfixed_angle_part = (-state_imag * decay_rate - shifted * frequency) / denominator
    return (state_real, state_imag, zoh_real, holdfixed_angle_part)


def input_maps(zoh_real, holdfixed_angle_part, input_real, input_imag):
    scale_real = zoh_real[None, :, :, None]
    scale_imag = holdfixed_angle_part[None, :, :, None]
    return (
        scale_real * input_real - scale_imag * input_imag,
        scale_real * input_imag + scale_imag * input_real,
    )


def pair_combine(earlier, later):
    mult_one_real, mult_one_imag, first_state_real, state_one_imag = earlier
    mult_two_real, second_multiplier_imag, state_two_real, state_two_imag = later
    return (
        mult_two_real * mult_one_real - second_multiplier_imag * mult_one_imag,
        mult_two_real * mult_one_imag + second_multiplier_imag * mult_one_real,
        mult_two_real * first_state_real - second_multiplier_imag * state_one_imag + state_two_real,
        mult_two_real * state_one_imag + second_multiplier_imag * first_state_real + state_two_imag,
    )


def blocked_scan(mult_real, mult_imag, drive_real, drive_imag, reverse):
    tokens_here, width = mult_real.shape
    span = min(16, tokens_here)
    count = tokens_here // span
    block_mr, block_mi, block_dr, block_di = (
        item.reshape(count, span, width) for item in (mult_real, mult_imag, drive_real, drive_imag)
    )
    running_pr = jnp.ones((count, width), jnp.float32)
    running_pi = jnp.zeros((count, width), jnp.float32)
    running_sr = jnp.zeros((count, width), jnp.float32)
    running_si = jnp.zeros((count, width), jnp.float32)
    slots = [None] * span
    positions = range(span - 1, -1, -1) if reverse else range(span)
    for place in positions:
        step_real = block_mr[:, place]
        step_imag = block_mi[:, place]
        running_pr, running_pi = (
            step_real * running_pr - step_imag * running_pi,
            step_real * running_pi + step_imag * running_pr,
        )
        running_sr, running_si = (
            step_real * running_sr - step_imag * running_si + block_dr[:, place],
            step_real * running_si + step_imag * running_sr + block_di[:, place],
        )
        slots[place] = (running_pr, running_pi, running_sr, running_si)
    inner = tuple((jnp.stack([slot[member] for slot in slots], axis=1) for member in range(4)))
    edge = 0 if reverse else span - 1
    ends = tuple((item[:, edge] for item in inner))
    outer = lax.associative_scan(pair_combine, ends, reverse=reverse, axis=0)
    ones_row = jnp.ones((1, width), jnp.float32)
    zero_row = jnp.zeros((1, width), jnp.float32)
    neutral = (ones_row, zero_row, zero_row, zero_row)
    if reverse:
        carry = tuple(
            (jnp.concatenate([item[1:], blank], axis=0) for item, blank in zip(outer, neutral))
        )
    else:
        carry = tuple(
            (jnp.concatenate([blank, item[:-1]], axis=0) for item, blank in zip(outer, neutral))
        )
    carry_mr, carry_mi, carry_sr, carry_si = (item[:, None, :] for item in carry)
    inner_mr, inner_mi, inner_sr, inner_si = inner
    prod_real = inner_mr * carry_mr - inner_mi * carry_mi
    prod_imag = inner_mr * carry_mi + inner_mi * carry_mr
    local_real = inner_sr + inner_mr * carry_sr - inner_mi * carry_si
    local_imag = inner_si + inner_mr * carry_si + inner_mi * carry_sr
    return tuple(
        (
            item.reshape(tokens_here, width)
            for item in (prod_real, prod_imag, local_real, local_imag)
        )
    )


def chain_combine(earlier, later):
    early_real, early_imag, early_state_real, early_state_imag, early_near, early_far = earlier
    late_real, late_imag, late_state_real, late_state_imag, late_near, late_far = later
    joined = (late_near == early_far) | (early_far < 0.0) | (late_near < 0.0)
    linked = jnp.where(joined, 1.0, 0.0).astype(jnp.float32)
    step_real = linked * late_real
    step_imag = linked * late_imag
    return (
        step_real * early_real - step_imag * early_imag,
        step_real * early_imag + step_imag * early_real,
        step_real * early_state_real - step_imag * early_state_imag + late_state_real,
        step_real * early_state_imag + step_imag * early_state_real + late_state_imag,
        jnp.where(early_near < 0.0, late_near, early_near),
        jnp.where(late_far < 0.0, early_far, late_far),
    )


def direction_pass(
    grouped,
    doc_ids,
    keep_rates,
    state_real,
    state_imag,
    map_real,
    map_imag,
    read_real,
    read_imag,
    reverse,
):
    tokens_here, groups_here, group_width = grouped.shape
    states_here = state_real.shape[1]
    flat_width = groups_here * states_here
    drive_real = jnp.einsum("tgi,gpi->tgp", grouped, map_real, precision=HIGHEST).reshape(
        tokens_here, flat_width
    )
    drive_imag = jnp.einsum("tgi,gpi->tgp", grouped, map_imag, precision=HIGHEST).reshape(
        tokens_here, flat_width
    )
    same_doc = (doc_ids[1:] == doc_ids[:-1]).astype(jnp.float32)
    single = jnp.ones((1,), jnp.float32)
    doc_links = (
        jnp.concatenate([same_doc, single]) if reverse else jnp.concatenate([single, same_doc])
    )
    factor = keep_rates[:, :, None] * doc_links[:, None, None]
    mult_real = (factor * state_real[None]).reshape(tokens_here, flat_width)
    mult_imag = (factor * state_imag[None]).reshape(tokens_here, flat_width)
    prod_real, prod_imag, local_real, local_imag = blocked_scan(
        mult_real, mult_imag, drive_real, drive_imag, reverse
    )
    far_end = 0 if reverse else tokens_here - 1
    near_end = tokens_here - 1 if reverse else 0
    doc_values = doc_ids.astype(jnp.float32)
    summary = (
        prod_real[far_end],
        prod_imag[far_end],
        local_real[far_end],
        local_imag[far_end],
        doc_values[near_end],
        doc_values[far_end],
    )
    neutral = (
        jnp.ones((flat_width,), jnp.float32),
        jnp.zeros((flat_width,), jnp.float32),
        jnp.zeros((flat_width,), jnp.float32),
        jnp.zeros((flat_width,), jnp.float32),
        jnp.array(-1.0, jnp.float32),
        jnp.array(-1.0, jnp.float32),
    )
    carried = prefix(summary, "sp", chain_combine, neutral, reverse)
    joined = (doc_values[near_end] == carried[5]).astype(jnp.float32)
    enter_real = joined * carried[2]
    enter_imag = joined * carried[3]
    full_real = local_real + prod_real * enter_real[None] - prod_imag * enter_imag[None]
    full_imag = local_imag + prod_real * enter_imag[None] + prod_imag * enter_real[None]
    result = jnp.einsum(
        "tgp,gip->tgi",
        full_real.reshape(tokens_here, groups_here, states_here),
        read_real,
        precision=HIGHEST,
    )
    result = result - jnp.einsum(
        "tgp,gip->tgi",
        full_imag.reshape(tokens_here, groups_here, states_here),
        read_imag,
        precision=HIGHEST,
    )
    return result.reshape(tokens_here, groups_here * group_width)


def rounded_sum(activations, weights, pieces):
    block_width = activations.shape[1] // pieces
    summed = jnp.zeros((activations.shape[0], weights.shape[1]), jnp.float32)
    for number in range(pieces):
        lower = number * block_width
        partial_value = jnp.dot(
            activations[:, lower : lower + block_width],
            weights[lower : lower + block_width],
            preferred_element_type=jnp.float32,
        ).astype(jnp.bfloat16)
        summed = summed + lax.optimization_barrier(partial_value).astype(jnp.float32)
    return summed


def local(
    mix_input,
    stream,
    doc_ids,
    log_dt,
    decay_rate,
    frequency,
    input_real,
    input_imag,
    output_real,
    output_imag,
    skip_gain,
    log_keep,
    proj_weight,
    norm_gain,
    gate_weight,
    up_weight,
    down_weight,
):
    state_real, state_imag, zoh_real, holdfixed_angle_part = discretize(
        log_dt, decay_rate, frequency
    )
    map_real, map_imag = input_maps(zoh_real, holdfixed_angle_part, input_real, input_imag)
    tokens_here = mix_input.shape[0]
    channels = mix_input.astype(jnp.float32)
    grouped = channels.reshape(tokens_here, log_dt.shape[0], GROUP)
    keep_rates = jnp.exp(log_keep).T
    mixed_pre = skip_gain * channels
    for direction, reverse in ((0, False), (1, True)):
        mixed_pre = mixed_pre + direction_pass(
            grouped,
            doc_ids,
            keep_rates,
            state_real,
            state_imag,
            map_real[direction],
            map_imag[direction],
            output_real[direction],
            output_imag[direction],
            reverse,
        )
    mixed = jax.nn.gelu(mixed_pre).astype(jnp.bfloat16)
    tp_size = lax.axis_size("tp")
    spread = lax.all_to_all(mixed, "tp", split_axis=0, concat_axis=1, tiled=True)
    proj_whole = lax.all_gather(proj_weight, "tp", axis=0, tiled=True)
    branch = rounded_sum(spread, proj_whole, tp_size)
    resid = stream.astype(jnp.float32) + branch
    scale = lax.rsqrt(jnp.mean(resid * resid, axis=-1, keepdims=True) + 1e-06)
    normed = (resid * scale * norm_gain).astype(jnp.bfloat16)
    rows_all = lax.all_gather(normed, "tp", axis=0, tiled=True)
    gate = jnp.dot(
        rows_all,
        lax.all_gather(gate_weight, "sp", axis=0, tiled=True),
        preferred_element_type=jnp.float32,
    )
    upward = jnp.dot(
        rows_all,
        lax.all_gather(up_weight, "sp", axis=0, tiled=True),
        preferred_element_type=jnp.float32,
    )
    hidden = (jax.nn.silu(gate) * upward).astype(jnp.bfloat16)
    partial_out = jnp.dot(
        hidden,
        lax.all_gather(down_weight, "sp", axis=1, tiled=True),
        preferred_element_type=jnp.float32,
    )
    ffn = lax.psum_scatter(
        partial_out.astype(jnp.bfloat16), "tp", scatter_dimension=0, tiled=True
    ).astype(jnp.float32)
    return (resid + 0.5 * ffn).astype(jnp.bfloat16)


def solution(mesh):
    placed = (
        P("sp", "tp"),
        P(("sp", "tp"), None),
        P("sp"),
        P("tp"),
        P("tp", None),
        P("tp", None),
        P(None, "tp", None, None),
        P(None, "tp", None, None),
        P(None, "tp", None, None),
        P(None, "tp", None, None),
        P("tp"),
        P("tp", "sp"),
        P("tp", None),
        P(),
        P("sp", "tp"),
        P("sp", "tp"),
        P("tp", "sp"),
    )
    return jax.shard_map(
        local, mesh=mesh, in_specs=placed, out_specs=P(("sp", "tp"), None), check_vma=False
    )
```

profile of v0, /device:TPU:0, one launch (start us, length us, event | category | flops | bytes accessed | tf_op | source)
XLA Modules:
  0.0 1120.7 jit_solution(13826116521377662551)
XLA Ops:
  21.2 2.5 copy.440
  25.2 6.5 fusion.197
  31.7 2.5 copy.438
  35.9 6.7 fusion.198
  42.5 2.6 copy.488
  46.6 5.8 fusion.199
  131.7 2.5 constant_dynamic-update-slice_fusion.95
  150.8 4.3 slice.1211
  155.1 3.9 slice.1221
  159.0 3.9 slice.1207
  162.9 3.9 slice.1219
  166.8 3.9 slice.1214
  170.7 3.9 slice.1227
  174.6 3.9 slice.1209
  178.5 3.9 slice.1216
  221.4 3.3 constant_dynamic-update-slice_fusion.79
  240.9 1.7 constant_dynamic-update-slice_fusion.12
  251.0 1.8 constant_dynamic-update-slice_fusion.6
  286.6 3.6 multiply_subtract_fusion.5
  291.9 1.7 add.3546
  294.4 32.4 %all-gather.3 = f32[8,1,1024]{2,1,0:T(1,128)S(1)} all-gather(f32[1,1,1024]{2,1,0:T(1,128)S(1)} %slice_bitcast_fusion.12), channel_id=1, replica_groups=mesh['sp'=8,'tp'=4] {'sp'}, dimensions={0}, use_global_device_ids=true | all-gather | bytes 36864 | tf_op jit(solution)/shard_map/all_gather | solution.py:14
  326.7 2.9 copy.472
  329.6 2.8 sub.1609
  333.2 30.6 %all-gather.2 = f32[8,1,1024]{2,1,0:T(1,128)S(1)} all-gather(f32[1,1,1024]{2,1,0:T(1,128)S(1)} %slice_bitcast_fusion.13), channel_id=1, replica_groups=mesh['sp'=8,'tp'=4] {'sp'}, dimensions={0}, use_global_device_ids=true | all-gather | bytes 36864 | tf_op jit(solution)/shard_map/all_gather | solution.py:14
  363.8 2.8 copy.475
  366.6 2.9 add.3545
  370.2 30.6 %all-gather.1 = f32[8,1,1024]{2,1,0:T(1,128)S(1)} all-gather(f32[1,1,1024]{2,1,0:T(1,128)S(1)} %slice_bitcast_fusion.14), channel_id=1, replica_groups=mesh['sp'=8,'tp'=4] {'sp'}, dimensions={0}, use_global_device_ids=true | all-gather | bytes 36864 | tf_op jit(solution)/shard_map/all_gather | solution.py:14
  400.8 2.8 copy.473
  403.8 2.8 sub.1615
  407.4 30.6 %all-gather = f32[8,1,1024]{2,1,0:T(1,128)S(1)} all-gather(f32[1,1,1024]{2,1,0:T(1,128)S(1)} %slice_bitcast_fusion.15), channel_id=1, replica_groups=mesh['sp'=8,'tp'=4] {'sp'}, dimensions={0}, use_global_device_ids=true | all-gather | bytes 36864 | tf_op jit(solution)/shard_map/all_gather | solution.py:14
  440.8 21.3 %all-reduce.74 = (f32[8]{0:T(128)S(1)}, f32[8]{0:T(128)S(1)}) all-reduce(f32[8]{0:T(128)S(1)} %slice_dynamic-update-slice_fusion, f32[8]{0:T(128)S(1)} %get-tuple-element.1051), channel_id=1, replica_groups=mesh['sp'=8,'tp'=4] {'sp'}, use_global_device_ids=true, to_apply=%add.73 | all-reduce | flops 16 | bytes 128
  462.1 27.3 %while.38 = (s32[]{:T(128)}, f32[1024]{0:T(1024)S(1)}, f32[1024]{0:T(1024)S(1)}, f32[]{:T(128)}, s32[]{:T(128)}, /*index=5*/f32[8]{0:T(128)S(1)}, f32[8,1024]{1,...) while((s32[]{:T(128)}, f32[1024]{0:T(1024)S(1)}, ...), condition=%wide.region_1.2_spmd.clone, body=%wide.region_0.1_spmd.clone.sunk | while | flops 14349 | bytes 65814 | solution.py:27
  493.7 2.5 slice.1291
  496.2 2.0 pad.529
  499.6 2.0 pad.344
  503.1 4.0 slice.1288
  547.3 2.4 slice.1268
  554.1 4.0 slice.1273
  583.4 3.8 multiply_subtract_fusion.3
  589.8 2.5 fusion.5
  592.3 3.2 fusion.9
  597.2 30.6 %all-gather.7 = f32[8,1,1024]{2,1,0:T(1,128)S(1)} all-gather(f32[1,1,1024]{2,1,0:T(1,128)S(1)} %slice_bitcast_fusion.8), channel_id=1, replica_groups=mesh['sp'=8,'tp'=4] {'sp'}, dimensions={0}, use_global_device_ids=true | all-gather | bytes 36864 | tf_op jit(solution)/shard_map/all_gather | solution.py:14
  627.8 1.8 copy.520
  629.6 1.9 sub.1696
  631.5 30.8 %all-gather.6 = f32[8,1,1024]{2,1,0:T(1,128)S(1)} all-gather(f32[1,1,1024]{2,1,0:T(1,128)S(1)} %slice_bitcast_fusion.9), channel_id=1, replica_groups=mesh['sp'=8,'tp'=4] {'sp'}, dimensions={0}, use_global_device_ids=true | all-gather | bytes 36864 | tf_op jit(solution)/shard_map/all_gather | solution.py:14
  662.3 1.8 copy.523
  664.2 2.0 add.3729
  666.1 30.6 %all-gather.5 = f32[8,1,1024]{2,1,0:T(1,128)S(1)} all-gather(f32[1,1,1024]{2,1,0:T(1,128)S(1)} %slice_bitcast_fusion.10), channel_id=1, replica_groups=mesh['sp'=8,'tp'=4] {'sp'}, dimensions={0}, use_global_device_ids=true | all-gather | bytes 36864 | tf_op jit(solution)/shard_map/all_gather | solution.py:14
  696.7 1.8 copy.521
  698.6 1.9 sub.1702
  700.4 30.6 %all-gather.4 = f32[8,1,1024]{2,1,0:T(1,128)S(1)} all-gather(f32[1,1,1024]{2,1,0:T(1,128)S(1)} %slice_bitcast_fusion.11), channel_id=1, replica_groups=mesh['sp'=8,'tp'=4] {'sp'}, dimensions={0}, use_global_device_ids=true | all-gather | bytes 36864 | tf_op jit(solution)/shard_map/all_gather | solution.py:14
  731.1 31.1 %while.39 = (s32[]{:T(128)}, f32[1024]{0:T(1024)S(1)}, f32[1024]{0:T(1024)S(1)}, f32[]{:T(128)}, s32[]{:T(128)}, /*index=5*/f32[8]{0:T(128)S(1)}, f32[8,1024]{1,...) while((s32[]{:T(128)}, f32[1024]{0:T(1024)S(1)}, ...), condition=%wide.region_3.4_spmd.clone, body=%wide.region_2.3_spmd.clone.sunk | while | flops 14353 | bytes 65876 | solution.py:27
  763.0 3.5 multiply_subtract_fusion
  766.4 2.5 fusion.1
  768.9 2.5 fusion.12
  771.7 7.2 all_to_all.19
  788.5 11.0 all-gather.16.cloned.1.call-done
  799.5 94.5 %all-gather.18.cloned.1.call-done = bf16[2048,1408]{1,0:T(8,128)(2,1)} async-done(((bf16[256,1408]{1,0:T(8,128)(2,1)}), bf16[2048,1408]{1,0:T(8,128)(2,1)}) %all-gather.18.cloned.1.call-update) | async-done | bytes 5767184 | tf_op jit(solution)/shard_map/all_gather | solution.py:272
  894.0 4.8 fusion.202
  898.8 87.8 %all-gather.20.cloned.1.call-done = bf16[2048,1408]{1,0:T(8,128)(2,1)} async-done(((bf16[256,1408]{1,0:T(8,128)(2,1)}), bf16[2048,1408]{1,0:T(8,128)(2,1)}) %all-gather.20.cloned.1.call-update) | async-done | bytes 5767184 | tf_op jit(solution)/shard_map/all_gather | solution.py:277
  986.6 93.2 %all-gather.22.cloned.1.call-done = bf16[1408,2048]{1,0:T(8,128)(2,1)} async-done(((bf16[1408,256]{1,0:T(8,128)(2,1)}), bf16[1408,2048]{1,0:T(8,128)(2,1)}) %all-gather.22.cloned.1.call-update) | async-done | bytes 5767184 | tf_op jit(solution)/shard_map/all_gather | solution.py:283
  1079.8 8.8 convolution_convert_fusion
  1088.6 23.1 %reduce-scatter.2.cloned.1.call-done = bf16[64,2048]{1,0:T(8,128)(2,1)} async-done(((bf16[256,2048]{1,0:T(8,128)(2,1)}), bf16[64,2048]{1,0:T(8,128)(2,1)}) %reduce-scatter.2.cloned.1.call-update) | async-done | bytes 262160 | tf_op jit(solution)/shard_map/reduce_scatter | solution.py:286
  1111.7 1.7 add_convert_fusion
  (878 shorter events, 327.0 us)
Async XLA Ops:
  6.5 772.4 %all-gather.14.cloned.1.call-start = ((), (), s32[]{:S(2)}) async-start(), calls=%async_computation.2 | async-start | bytes 5242880 | tf_op jit(solution)/shard_map/all_gather | solution.py:264
  7.3 792.2 %all-gather.16.cloned.1.call-start = ((), (), s32[]{:S(2)}) async-start(), calls=%async_computation.3 | async-start | bytes 1310720 | tf_op jit(solution)/shard_map/all_gather | solution.py:269
  57.5 181.7 %copy-start = (f32[16,16,1024]{2,0,1:T(8,128)}, f32[16,16,1024]{2,0,1:T(8,128)S(1)}, u32[]{:S(2)}) copy-start(f32[16,16,1024]{2,0,1:T(8,128)S(1)} %get-tuple-element.1046) | copy-start | bytes 3145732
  57.5 181.7 %copy-start.2 = (f32[16,16,1024]{2,0,1:T(8,128)}, f32[16,16,1024]{2,0,1:T(8,128)S(1)}, u32[]{:S(2)}) copy-start(f32[16,16,1024]{2,0,1:T(8,128)S(1)} %get-tuple-element.1047) | copy-start | bytes 3145732
  224.7 17.9 %copy-start.88 = (f32[16,1,1024]{2,1,0:T(1,128)S(1)}, f32[16,1,1024]{2,1,0:T(1,128)}, u32[]{:S(2)}) copy-start(f32[16,1,1024]{2,1,0:T(1,128)} %get-tuple-element.876) | copy-start | bytes 196612
  224.7 19.5 %copy-start.84 = (f32[16,1,1024]{2,1,0:T(1,128)S(1)}, f32[16,1,1024]{2,1,0:T(1,128)}, u32[]{:S(2)}) copy-start(f32[16,1,1024]{2,1,0:T(1,128)} %get-tuple-element.875) | copy-start | bytes 196612
  224.7 19.5 %copy-start.93 = (f32[16,1,1024]{2,1,0:T(1,128)S(1)}, f32[16,1,1024]{2,1,0:T(1,128)}, u32[]{:S(2)}) copy-start(f32[16,1,1024]{2,1,0:T(1,128)} %get-tuple-element.890) | copy-start | bytes 196612
  403.7 34.3 %copy-start.180 = (u32[32]{0:T(128)S(1)}, u32[32]{0:T(128)}, u32[]{:S(2)}) copy-start(u32[32]{0:T(128)} %constant.276) | copy-start | bytes 388
  403.7 34.9 %copy-start.177 = (f32[256]{0:T(256)S(1)}, f32[256]{0:T(256)}, u32[]{:S(2)}) copy-start(f32[256]{0:T(256)} %convert_element_type.65) | copy-start | bytes 3076
  403.7 87.9 %copy-start.146 = (f32[7,1024]{1,0:T(8,128)S(1)}, f32[7,1024]{1,0:T(8,128)}, u32[]{:S(2)}) copy-start(f32[7,1024]{1,0:T(8,128)} %slice.1260) | copy-start | bytes 86020
  403.7 88.0 %copy-start.145 = (f32[7,1024]{1,0:T(8,128)S(1)}, f32[7,1024]{1,0:T(8,128)}, u32[]{:S(2)}) copy-start(f32[7,1024]{1,0:T(8,128)} %slice.1204) | copy-start | bytes 86020
  403.7 88.3 %copy-start.167 = (f32[1,1024]{1,0:T(1,128)S(1)}, f32[1,1024]{1,0:T(1,128)}, u32[]{:S(2)}) copy-start(f32[1,1024]{1,0:T(1,128)} %get-tuple-element.1041) | copy-start | bytes 12292
  403.7 88.3 %copy-start.171 = (f32[1,1024]{1,0:T(1,128)S(1)}, f32[1,1024]{1,0:T(1,128)}, u32[]{:S(2)}) copy-start(f32[1,1024]{1,0:T(1,128)} %get-tuple-element.1006) | copy-start | bytes 12292
  403.7 88.3 %copy-start.155 = (f32[2,1024]{1,0:T(2,128)S(1)}, f32[2,1024]{1,0:T(2,128)}, u32[]{:S(2)}) copy-start(f32[2,1024]{1,0:T(2,128)} %pad_add_fusion) | copy-start | bytes 24580
  403.7 88.3 %copy-start.156 = (f32[2,1024]{1,0:T(2,128)S(1)}, f32[2,1024]{1,0:T(2,128)}, u32[]{:S(2)}) copy-start(f32[2,1024]{1,0:T(2,128)} %pad_add_fusion.1) | copy-start | bytes 24580
  403.7 88.4 %copy-start.166 = (f32[1,1024]{1,0:T(1,128)S(1)}, f32[1,1024]{1,0:T(1,128)}, u32[]{:S(2)}) copy-start(f32[1,1024]{1,0:T(1,128)} %get-tuple-element.1040) | copy-start | bytes 12292
  403.7 88.4 %copy-start.170 = (f32[1,1024]{1,0:T(1,128)S(1)}, f32[1,1024]{1,0:T(1,128)}, u32[]{:S(2)}) copy-start(f32[1,1024]{1,0:T(1,128)} %get-tuple-element.1007) | copy-start | bytes 12292
  403.7 88.4 %copy-start.138 = (f32[3,1024]{1,0:T(4,128)S(1)}, f32[3,1024]{1,0:T(4,128)}, u32[]{:S(2)}) copy-start(f32[3,1024]{1,0:T(4,128)} %slice.1222) | copy-start | bytes 36868
  403.7 88.4 %copy-start.140 = (f32[3,1024]{1,0:T(4,128)S(1)}, f32[3,1024]{1,0:T(4,128)}, u32[]{:S(2)}) copy-start(f32[3,1024]{1,0:T(4,128)} %slice.1254) | copy-start | bytes 36868
  403.7 88.5 %copy-start.164 = (f32[1,1024]{1,0:T(1,128)S(1)}, f32[1,1024]{1,0:T(1,128)}, u32[]{:S(2)}) copy-start(f32[1,1024]{1,0:T(1,128)} %slice.1534) | copy-start | bytes 12292
  403.8 88.6 %copy-start.163 = (f32[1,1024]{1,0:T(1,128)S(1)}, f32[1,1024]{1,0:T(1,128)}, u32[]{:S(2)}) copy-start(f32[1,1024]{1,0:T(1,128)} %slice.1519) | copy-start | bytes 12292
  403.8 89.9 %copy-start.162 = (f32[1,1024]{1,0:T(1,128)S(1)}, f32[1,1024]{1,0:T(1,128)}, u32[]{:S(2)}) copy-start(f32[1,1024]{1,0:T(1,128)} %slice.1537) | copy-start | bytes 12292
  406.6 91.6 %copy-start.161 = (f32[1,1024]{1,0:T(1,128)S(1)}, f32[1,1024]{1,0:T(1,128)}, u32[]{:S(2)}) copy-start(f32[1,1024]{1,0:T(1,128)} %slice.1518) | copy-start | bytes 12292
  493.7 42.4 %copy-start.108 = (f32[16,1,1024]{2,0,1:T(8,128)S(1)}, f32[16,1,1024]{2,0,1:T(8,128)}, u32[]{:S(2)}) copy-start(f32[16,1,1024]{2,0,1:T(8,128)} %get-tuple-element.812) | copy-start | bytes 196612
  496.2 40.6 %copy-start.107 = (f32[16,1,1024]{2,0,1:T(8,128)S(1)}, f32[16,1,1024]{2,0,1:T(8,128)}, u32[]{:S(2)}) copy-start(f32[16,1,1024]{2,0,1:T(8,128)} %get-tuple-element.815) | copy-start | bytes 196612
  498.2 39.2 %copy-start.43 = (f32[16,1,1024]{2,0,1:T(8,128)S(1)}, f32[16,1,1024]{2,0,1:T(8,128)}, u32[]{:S(2)}) copy-start(f32[16,1,1024]{2,0,1:T(8,128)} %get-tuple-element.715) | copy-start | bytes 196612
  498.2 39.2 %copy-start.54 = (f32[16,1,1024]{2,1,0:T(1,128)S(1)}, f32[16,1,1024]{2,1,0:T(1,128)}, u32[]{:S(2)}) copy-start(f32[16,1,1024]{2,1,0:T(1,128)} %get-tuple-element.898) | copy-start | bytes 196612
  507.1 22.8 %copy-start.118 = (f32[16,1,1024]{2,0,1:T(8,128)S(1)}, f32[16,1,1024]{2,0,1:T(8,128)}, u32[]{:S(2)}) copy-start(f32[16,1,1024]{2,0,1:T(8,128)} %get-tuple-element.792) | copy-start | bytes 196612
  507.1 23.4 %copy-start.117 = (f32[16,1,1024]{2,0,1:T(8,128)S(1)}, f32[16,1,1024]{2,0,1:T(8,128)}, u32[]{:S(2)}) copy-start(f32[16,1,1024]{2,0,1:T(8,128)} %get-tuple-element.795) | copy-start | bytes 196612
  507.1 24.0 %copy-start.116 = (f32[16,1,1024]{2,0,1:T(8,128)S(1)}, f32[16,1,1024]{2,0,1:T(8,128)}, u32[]{:S(2)}) copy-start(f32[16,1,1024]{2,0,1:T(8,128)} %get-tuple-element.796) | copy-start | bytes 196612
  507.1 24.6 %copy-start.115 = (f32[16,1,1024]{2,0,1:T(8,128)S(1)}, f32[16,1,1024]{2,0,1:T(8,128)}, u32[]{:S(2)}) copy-start(f32[16,1,1024]{2,0,1:T(8,128)} %get-tuple-element.799) | copy-start | bytes 196612
  507.1 25.3 %copy-start.114 = (f32[16,1,1024]{2,0,1:T(8,128)S(1)}, f32[16,1,1024]{2,0,1:T(8,128)}, u32[]{:S(2)}) copy-start(f32[16,1,1024]{2,0,1:T(8,128)} %get-tuple-element.800) | copy-start | bytes 196612
  507.1 25.9 %copy-start.113 = (f32[16,1,1024]{2,0,1:T(8,128)S(1)}, f32[16,1,1024]{2,0,1:T(8,128)}, u32[]{:S(2)}) copy-start(f32[16,1,1024]{2,0,1:T(8,128)} %get-tuple-element.803) | copy-start | bytes 196612
  507.1 26.5 %copy-start.112 = (f32[16,1,1024]{2,0,1:T(8,128)S(1)}, f32[16,1,1024]{2,0,1:T(8,128)}, u32[]{:S(2)}) copy-start(f32[16,1,1024]{2,0,1:T(8,128)} %get-tuple-element.804) | copy-start | bytes 196612
  507.2 27.1 %copy-start.111 = (f32[16,1,1024]{2,0,1:T(8,128)S(1)}, f32[16,1,1024]{2,0,1:T(8,128)}, u32[]{:S(2)}) copy-start(f32[16,1,1024]{2,0,1:T(8,128)} %get-tuple-element.807) | copy-start | bytes 196612
  507.2 27.7 %copy-start.110 = (f32[16,1,1024]{2,0,1:T(8,128)S(1)}, f32[16,1,1024]{2,0,1:T(8,128)}, u32[]{:S(2)}) copy-start(f32[16,1,1024]{2,0,1:T(8,128)} %get-tuple-element.808) | copy-start | bytes 196612
  507.2 28.3 %copy-start.109 = (f32[16,1,1024]{2,0,1:T(8,128)S(1)}, f32[16,1,1024]{2,0,1:T(8,128)}, u32[]{:S(2)}) copy-start(f32[16,1,1024]{2,0,1:T(8,128)} %get-tuple-element.811) | copy-start | bytes 196612
  507.2 30.2 %copy-start.132 = (f32[16,1,1024]{2,0,1:T(8,128)S(1)}, f32[16,1,1024]{2,0,1:T(8,128)}, u32[]{:S(2)}) copy-start(f32[16,1,1024]{2,0,1:T(8,128)} %get-tuple-element.716) | copy-start | bytes 196612
  510.9 28.7 %copy-start.144 = (f32[7,1024]{1,0:T(8,128)S(1)}, f32[7,1024]{1,0:T(8,128)}, u32[]{:S(2)}) copy-start(f32[7,1024]{1,0:T(8,128)} %slice.1270) | copy-start | bytes 86020
  510.9 28.9 %copy-start.143 = (f32[7,1024]{1,0:T(8,128)S(1)}, f32[7,1024]{1,0:T(8,128)}, u32[]{:S(2)}) copy-start(f32[7,1024]{1,0:T(8,128)} %slice.1265) | copy-start | bytes 86020
  515.3 27.7 %copy-start.139 = (f32[3,1024]{1,0:T(4,128)S(1)}, f32[3,1024]{1,0:T(4,128)}, u32[]{:S(2)}) copy-start(f32[3,1024]{1,0:T(4,128)} %slice.1222) | copy-start | bytes 36868
  544.4 37.0 %copy-start.11 = (f32[16,16,1024]{2,0,1:T(8,128)S(1)}, f32[16,16,1024]{2,0,1:T(8,128)}, u32[]{:S(2)}) copy-start(f32[16,16,1024]{2,0,1:T(8,128)} %get-tuple-element.991) | copy-start | bytes 3145732
  547.2 36.0 %copy-start.124 = (f32[16,1,1024]{2,0,1:T(8,128)S(1)}, f32[16,1,1024]{2,0,1:T(8,128)}, u32[]{:S(2)}) copy-start(f32[16,1,1024]{2,0,1:T(8,128)} %get-tuple-element.733) | copy-start | bytes 196612
  547.3 36.0 %copy-start.123 = (f32[16,1,1024]{2,0,1:T(8,128)S(1)}, f32[16,1,1024]{2,0,1:T(8,128)}, u32[]{:S(2)}) copy-start(f32[16,1,1024]{2,0,1:T(8,128)} %get-tuple-element.736) | copy-start | bytes 196612
  549.7 33.6 %copy-start.122 = (f32[16,1,1024]{2,0,1:T(8,128)S(1)}, f32[16,1,1024]{2,0,1:T(8,128)}, u32[]{:S(2)}) copy-start(f32[16,1,1024]{2,0,1:T(8,128)} %get-tuple-element.737) | copy-start | bytes 196612
  550.5 32.8 %copy-start.121 = (f32[16,1,1024]{2,0,1:T(8,128)S(1)}, f32[16,1,1024]{2,0,1:T(8,128)}, u32[]{:S(2)}) copy-start(f32[16,1,1024]{2,0,1:T(8,128)} %get-tuple-element.740) | copy-start | bytes 196612
  552.6 30.7 %copy-start.120 = (f32[16,1,1024]{2,0,1:T(8,128)S(1)}, f32[16,1,1024]{2,0,1:T(8,128)}, u32[]{:S(2)}) copy-start(f32[16,1,1024]{2,0,1:T(8,128)} %get-tuple-element.741) | copy-start | bytes 196612
  554.1 29.2 %copy-start.119 = (f32[16,1,1024]{2,0,1:T(8,128)S(1)}, f32[16,1,1024]{2,0,1:T(8,128)}, u32[]{:S(2)}) copy-start(f32[16,1,1024]{2,0,1:T(8,128)} %get-tuple-element.744) | copy-start | bytes 196612
  558.2 24.9 %copy-start.130 = (f32[16,1,1024]{2,0,1:T(8,128)S(1)}, f32[16,1,1024]{2,0,1:T(8,128)}, u32[]{:S(2)}) copy-start(f32[16,1,1024]{2,0,1:T(8,128)} %get-tuple-element.721) | copy-start | bytes 196612
  558.2 24.9 %copy-start.129 = (f32[16,1,1024]{2,0,1:T(8,128)S(1)}, f32[16,1,1024]{2,0,1:T(8,128)}, u32[]{:S(2)}) copy-start(f32[16,1,1024]{2,0,1:T(8,128)} %get-tuple-element.724) | copy-start | bytes 196612
  558.2 24.9 %copy-start.128 = (f32[16,1,1024]{2,0,1:T(8,128)S(1)}, f32[16,1,1024]{2,0,1:T(8,128)}, u32[]{:S(2)}) copy-start(f32[16,1,1024]{2,0,1:T(8,128)} %get-tuple-element.725) | copy-start | bytes 196612
  558.2 25.0 %copy-start.127 = (f32[16,1,1024]{2,0,1:T(8,128)S(1)}, f32[16,1,1024]{2,0,1:T(8,128)}, u32[]{:S(2)}) copy-start(f32[16,1,1024]{2,0,1:T(8,128)} %get-tuple-element.728) | copy-start | bytes 196612
  558.2 25.0 %copy-start.126 = (f32[16,1,1024]{2,0,1:T(8,128)S(1)}, f32[16,1,1024]{2,0,1:T(8,128)}, u32[]{:S(2)}) copy-start(f32[16,1,1024]{2,0,1:T(8,128)} %get-tuple-element.729) | copy-start | bytes 196612
  558.2 25.0 %copy-start.125 = (f32[16,1,1024]{2,0,1:T(8,128)S(1)}, f32[16,1,1024]{2,0,1:T(8,128)}, u32[]{:S(2)}) copy-start(f32[16,1,1024]{2,0,1:T(8,128)} %get-tuple-element.732) | copy-start | bytes 196612
  558.2 25.2 %copy-start.12 = (f32[16,16,1024]{2,0,1:T(8,128)S(1)}, f32[16,16,1024]{2,0,1:T(8,128)}, u32[]{:S(2)}) copy-start(f32[16,16,1024]{2,0,1:T(8,128)} %get-tuple-element.863) | copy-start | bytes 3145732
  558.2 25.2 %copy-start.13 = (f32[16,16,1024]{2,0,1:T(8,128)S(1)}, f32[16,16,1024]{2,0,1:T(8,128)}, u32[]{:S(2)}) copy-start(f32[16,16,1024]{2,0,1:T(8,128)} %get-tuple-element.862) | copy-start | bytes 3145732
  558.2 25.2 %copy-start.131 = (f32[16,1024]{1,0:T(8,128)S(1)}, f32[16,1024]{1,0:T(8,128)}, u32[]{:S(2)}) copy-start(f32[16,1024]{1,0:T(8,128)} %concatenate.133) | copy-start | bytes 196612
  698.6 32.5 %copy-start.182 = (f32[8]{0:T(128)S(1)}, f32[8]{0:T(128)}, u32[]{:S(2)}) copy-start(f32[8]{0:T(128)} %copy-done.181) | copy-start | bytes 100
  698.6 32.5 %copy-start.184 = (f32[8]{0:T(128)S(1)}, f32[8]{0:T(128)}, u32[]{:S(2)}) copy-start(f32[8]{0:T(128)} %copy-done.183) | copy-start | bytes 100
  786.3 107.7 %all-gather.18.cloned.1.call-start = ((), (), s32[]{:S(2)}) async-start(), calls=%async_computation.4 | async-start | bytes 6488064 | tf_op jit(solution)/shard_map/all_gather | solution.py:272
  787.0 199.5 %all-gather.20.cloned.1.call-start = ((), (), s32[]{:S(2)}) async-start(), calls=%async_computation.5 | async-start | bytes 6488064 | tf_op jit(solution)/shard_map/all_gather | solution.py:277
  787.6 292.2 %all-gather.22.cloned.1.call-start = ((), (), s32[]{:S(2)}) async-start(), calls=%async_computation.6 | async-start | bytes 6488064 | tf_op jit(solution)/shard_map/all_gather | solution.py:283
  788.2 323.5 %reduce-scatter.2.cloned.1.call-start = ((), (), s32[]{:S(2)}) async-start(), calls=%async_computation.7 | async-start | bytes 1310720 | tf_op jit(solution)/shard_map/reduce_scatter | solution.py:286
  799.5 280.3 %copy-start.179 = (bf16[256,2048]{1,0:T(8,128)(2,1)S(1)}, bf16[256,2048]{1,0:T(8,128)(2,1)}, u32[]{:S(2)}) copy-start(bf16[256,2048]{1,0:T(8,128)(2,1)} %all-gather.16.cloned.1.call-done) | copy-start | bytes 3145732
  (127 other events, 538.9 us)
Sparse Core Ops, SparseCore 0:
  8.9 37.1 all-gather.13
  786.4 13.0 all-gather.15
  801.6 92.2 all-gather.17
  896.0 90.4 all-gather.19
  988.4 91.2 all-gather.21
  1088.7 22.9 reduce-scatter.1
where the time goes:
time: 1140 us; the launch traced here: 1120 us
  local copies, waits for them, and re-layouts  328 us (29%)
  waiting for transfers between devices  312 us (27%)
  blocking collectives  275 us (24%)
  other arithmetic  112 us (10%)
  loops' own time  39.4 us (3%)
  matrix products  35.7 us (3%)
  between operations  18.3 us (2%)
    all_gather x8, blocking collectives, prefix(): everything = jax.tree.map(lambda part: lax.all_gather(part, axis), array)  247 us
    slice x98, local copies, waits for them, and re-layouts, blocked_scan(): outer = lax.associative_scan(pair_combine, ends, reverse=reverse, axis=0)  141 us
    all_gather x1, waiting for transfers between devices, local(): lax.all_gather(gate_weight, 'sp', axis=0, tiled=True)  94.5 us
    all_gather x1, waiting for transfers between devices, local(): lax.all_gather(down_weight, 'sp', axis=1, tiled=True)  93.2 us
    all_gather x1, waiting for transfers between devices, local(): lax.all_gather(up_weight, 'sp', axis=0, tiled=True)  87.8 us
    unnamed x455, local copies, waits for them, and re-layouts  66.1 us
    another operation x2, loops' own time, prefix(): return lax.fori_loop(0, devices, hop, start)  39.4 us
    unnamed x35, other arithmetic  37.9 us
  transfers between devices with their start and end apart: 6, of which 5 were waited for; matrix products, arithmetic and copies ran while one was open for 40% of the time, Pallas kernels for 0%

commit v1 on v0

v1 whole, which is shorter than its diff:
```python
import functools

import jax
import jax.numpy as jnp
from jax import lax
from jax.experimental import pallas as pl
from jax.experimental.pallas import tpu as pltpu
from jax.sharding import PartitionSpec as P

GROUP = 16
CHUNKS = 8
BF = jnp.bfloat16
F32 = jnp.float32


def discretize(log_dt, decay_rate, frequency):
    step_size = jnp.exp(log_dt)[:, None]
    magnitude = jnp.exp(-step_size * decay_rate)
    angle_step = step_size * frequency
    state_real = magnitude * jnp.cos(angle_step)
    state_imag = magnitude * jnp.sin(angle_step)
    denominator = decay_rate * decay_rate + frequency * frequency
    shifted = state_real - 1.0
    zoh_real = (-shifted * decay_rate + state_imag * frequency) / denominator
    holdfixed_angle_part = (-state_imag * decay_rate - shifted * frequency) / denominator
    return (state_real, state_imag, zoh_real, holdfixed_angle_part)


def input_maps(zoh_real, holdfixed_angle_part, input_real, input_imag):
    scale_real = zoh_real[None, :, :, None]
    scale_imag = holdfixed_angle_part[None, :, :, None]
    return (
        scale_real * input_real - scale_imag * input_imag,
        scale_real * input_imag + scale_imag * input_real,
    )


def split(value):
    high = value.astype(BF)
    return high, (value - high.astype(F32)).astype(BF)


def dot_nt(left, right):
    return lax.dot_general(left, right, (((1,), (1,)), ((), ())), preferred_element_type=F32)


def one_hot(shape, row_of, lane_of):
    rows = lax.broadcasted_iota(jnp.int32, shape, 0)
    lanes = lax.broadcasted_iota(jnp.int32, shape, 1)
    return row_of(rows) == lane_of(lanes)


def spread_keep(keep, groups, states):
    pick = one_hot((groups, groups * states), lambda r: r, lambda c: c // states)
    pick = pick.astype(F32).astype(BF)
    first, rest = split(keep)
    rest32 = keep - first.astype(F32)
    second, third = split(rest32)
    return (
        jnp.dot(first, pick, preferred_element_type=F32)
        + jnp.dot(second, pick, preferred_element_type=F32)
        + jnp.dot(third, pick, preferred_element_type=F32)
    )


def cmul(ar, ai, br, bi):
    return ar * br - ai * bi, ar * bi + ai * br


def power(real, imag, count):
    result = None
    while count:
        if count & 1:
            result = (real, imag) if result is None else cmul(*result, real, imag)
        count >>= 1
        if count:
            real, imag = cmul(real, imag, real, imag)
    return result


def drive_kernel(
    u_ref, keep_ref, map_ref, pole_ref, doc_ref, drive_ref, chunk_ref, total_ref, factor_ref
):
    tokens, width = u_ref.shape
    flat = pole_ref.shape[1]
    groups = width // GROUP
    states = flat // groups
    span = tokens // CHUNKS
    u = u_ref[...]
    tile = one_hot((GROUP, width), lambda r: r, lambda c: c % GROUP).astype(F32).astype(BF)
    own = one_hot((flat, width), lambda r: r // states, lambda c: c // GROUP)
    for quarter in range(4):
        total = None
        for piece in split(map_ref[quarter]):
            wide = jnp.dot(piece, tile, preferred_element_type=F32)
            wide = jnp.where(own, wide, 0.0).astype(BF)
            part = dot_nt(u, wide)
            total = part if total is None else total + part
        drive_ref[quarter] = total
    pole_real = jnp.broadcast_to(pole_ref[0:1], (CHUNKS, flat))
    pole_imag = jnp.broadcast_to(pole_ref[1:2], (CHUNKS, flat))
    long_real, long_imag = power(pole_ref[0:1], pole_ref[1:2], span)
    for way in range(2):
        factor_ref[...] = spread_keep(keep_ref[way], groups, states)

        def step(k, carry):
            real, imag, kept = carry
            at = k if way == 0 else span - 1 - k
            rows = pl.ds(pl.multiple_of(at * CHUNKS, CHUNKS), CHUNKS)
            factor = factor_ref[rows]
            real, imag = factor * real, factor * imag
            real, imag = cmul(pole_real, pole_imag, real, imag)
            return (
                real + drive_ref[2 * way, rows],
                imag + drive_ref[2 * way + 1, rows],
                kept * factor,
            )

        zero = jnp.zeros((CHUNKS, flat), F32)
        real, imag, kept = lax.fori_loop(0, span, step, (zero, zero, zero + 1.0))
        mult_real, mult_imag = kept * long_real, kept * long_imag
        for number, item in enumerate((mult_real, mult_imag, real, imag)):
            chunk_ref[way, number] = item
        state = (jnp.zeros((1, flat), F32), jnp.zeros((1, flat), F32))
        product = (jnp.ones((1, flat), F32), jnp.zeros((1, flat), F32))
        for chunk in range(CHUNKS) if way == 0 else range(CHUNKS - 1, -1, -1):
            here = [chunk_ref[way, number, chunk : chunk + 1] for number in range(4)]
            product = cmul(here[0], here[1], *product)
            moved = cmul(here[0], here[1], *state)
            state = (moved[0] + here[2], moved[1] + here[3])
        for number, item in enumerate(product + state):
            total_ref[4 * way + number : 4 * way + number + 1] = item
    total_ref[8:9] = jnp.full((1, flat), doc_ref[0], F32)
    total_ref[9:10] = jnp.full((1, flat), doc_ref[1], F32)
    total_ref[10:16] = jnp.zeros((6, flat), F32)


def read_kernel(
    devices,
    u_ref,
    keep_ref,
    drive_ref,
    chunk_ref,
    all_ref,
    read_ref,
    pole_ref,
    skip_ref,
    doc_ref,
    me_ref,
    out_ref,
    factor_ref,
    start_ref,
    real_ref,
    imag_ref,
    y_ref,
):
    tokens, width = u_ref.shape
    flat = pole_ref.shape[1]
    groups = width // GROUP
    states = flat // groups
    span = tokens // CHUNKS
    me = me_ref[0]
    y_ref[...] = skip_ref[...] * u_ref[...].astype(F32)
    pole_real = jnp.broadcast_to(pole_ref[0:1], (CHUNKS, flat))
    pole_imag = jnp.broadcast_to(pole_ref[1:2], (CHUNKS, flat))
    tile = one_hot((states, flat), lambda r: r, lambda c: c % states).astype(F32).astype(BF)
    own = one_hot((width, flat), lambda r: r // GROUP, lambda c: c // states)
    for way in range(2):
        real = jnp.zeros((1, flat), F32)
        imag = jnp.zeros((1, flat), F32)
        edge = jnp.full((1, flat), -1.0, F32)
        for device in range(devices) if way == 0 else range(devices - 1, -1, -1):
            reached = jnp.full((1, flat), device, jnp.int32)
            reached = reached < me if way == 0 else reached > me
            row = [all_ref[device, 4 * way + k : 4 * way + k + 1] for k in range(4)]
            near = all_ref[device, 8 + way : 9 + way]
            far = all_ref[device, 9 - way : 10 - way]
            joined = jnp.where(near == edge, 1.0, 0.0)
            moved = cmul(row[0], row[1], joined * real, joined * imag)
            real = jnp.where(reached, moved[0] + row[2], real)
            imag = jnp.where(reached, moved[1] + row[3], imag)
            edge = jnp.where(reached, far, edge)
        joined = jnp.where(jnp.full((1, flat), doc_ref[way], F32) == edge, 1.0, 0.0)
        real, imag = joined * real, joined * imag
        for chunk in range(CHUNKS) if way == 0 else range(CHUNKS - 1, -1, -1):
            start_ref[0, chunk : chunk + 1] = real
            start_ref[1, chunk : chunk + 1] = imag
            here = [chunk_ref[way, number, chunk : chunk + 1] for number in range(4)]
            moved = cmul(here[0], here[1], real, imag)
            real, imag = moved[0] + here[2], moved[1] + here[3]
        factor_ref[...] = spread_keep(keep_ref[way], groups, states)

        def step(k, carry):
            real, imag = carry
            at = k if way == 0 else span - 1 - k
            rows = pl.ds(pl.multiple_of(at * CHUNKS, CHUNKS), CHUNKS)
            factor = factor_ref[rows]
            real, imag = factor * real, factor * imag
            real, imag = cmul(pole_real, pole_imag, real, imag)
            real = real + drive_ref[2 * way, rows]
            imag = imag + drive_ref[2 * way + 1, rows]
            real_ref[rows] = real
            imag_ref[rows] = imag
            return real, imag

        lax.fori_loop(0, span, step, (start_ref[0], start_ref[1]))
        for part, held in enumerate((real_ref, imag_ref)):
            high, low = split(held[...])
            read_high, read_low = split(read_ref[2 * way + part])
            wide_high = jnp.dot(read_high, tile, preferred_element_type=F32)
            wide_high = jnp.where(own, wide_high, 0.0).astype(BF)
            wide_low = jnp.dot(read_low, tile, preferred_element_type=F32)
            wide_low = jnp.where(own, wide_low, 0.0).astype(BF)
            y_ref[...] += (
                dot_nt(high, wide_high) + dot_nt(low, wide_high) + dot_nt(high, wide_low)
            )
    y = y_ref[...]
    inner = 0.7978845608028654 * (y + 0.044715 * (y * y * y))
    out_ref[...] = (0.5 * y * (1.0 + jnp.tanh(inner))).astype(BF)


def vmem(count):
    return [pl.BlockSpec(memory_space=pltpu.VMEM)] * count


def smem(count):
    return [pl.BlockSpec(memory_space=pltpu.SMEM)] * count


def interleave(array):
    tokens = array.shape[0]
    parts = array.reshape((CHUNKS, tokens // CHUNKS) + array.shape[1:])
    return jnp.swapaxes(parts, 0, 1).reshape(array.shape)


def deinterleave(array):
    tokens = array.shape[0]
    parts = array.reshape((tokens // CHUNKS, CHUNKS) + array.shape[1:])
    return jnp.swapaxes(parts, 0, 1).reshape(array.shape)


def mixing(
    mix_input, doc_ids, log_dt, decay_rate, frequency, input_real, input_imag,
    output_real, output_imag, skip_gain, log_keep,
):
    tokens, width = mix_input.shape
    groups, states = decay_rate.shape
    flat = groups * states
    pole_real, pole_imag, zoh_real, zoh_imag = discretize(log_dt, decay_rate, frequency)
    map_real, map_imag = input_maps(zoh_real, zoh_imag, input_real, input_imag)
    maps = jnp.stack([map_real, map_imag], 1).reshape(4, flat, GROUP)
    reads = jnp.stack([output_real, -output_imag], 1).reshape(4, width, states)
    poles = jnp.stack([pole_real.reshape(flat), pole_imag.reshape(flat)])
    same = (doc_ids[1:] == doc_ids[:-1]).astype(F32)
    one = jnp.ones((1,), F32)
    links = jnp.stack([jnp.concatenate([one, same]), jnp.concatenate([same, one])])
    keep = jnp.exp(log_keep).T[None] * links[:, :, None]
    keep = jnp.stack([interleave(keep[0]), interleave(keep[1])])
    u = interleave(mix_input)
    doc_edges = jnp.stack([doc_ids[0], doc_ids[-1]]).astype(F32)
    drive, chunk, total = pl.pallas_call(
        drive_kernel,
        out_shape=(
            jax.ShapeDtypeStruct((4, tokens, flat), F32),
            jax.ShapeDtypeStruct((2, 4, CHUNKS, flat), F32),
            jax.ShapeDtypeStruct((16, flat), F32),
        ),
        in_specs=vmem(4) + smem(1),
        out_specs=tuple(vmem(3)),
        scratch_shapes=[pltpu.VMEM((tokens, flat), F32)],
        compiler_params=pltpu.CompilerParams(vmem_limit_bytes=40 << 20),
        cost_estimate=pl.CostEstimate(flops=10**8, bytes_accessed=6 << 20, transcendentals=0),
        name="drive",
    )(u, keep, maps, poles, doc_edges)
    everything = lax.all_gather(total, "sp")
    devices = everything.shape[0]
    me = lax.axis_index("sp").astype(jnp.int32).reshape(1)
    mixed = pl.pallas_call(
        functools.partial(read_kernel, devices),
        out_shape=jax.ShapeDtypeStruct((tokens, width), BF),
        in_specs=vmem(8) + smem(2),
        out_specs=vmem(1)[0],
        scratch_shapes=[
            pltpu.VMEM((tokens, flat), F32),
            pltpu.VMEM((2, CHUNKS, flat), F32),
            pltpu.VMEM((tokens, flat), F32),
            pltpu.VMEM((tokens, flat), F32),
            pltpu.VMEM((tokens, width), F32),
        ],
        compiler_params=pltpu.CompilerParams(vmem_limit_bytes=40 << 20),
        cost_estimate=pl.CostEstimate(flops=10**8, bytes_accessed=6 << 20, transcendentals=0),
        name="read",
    )(u, keep, drive, chunk, everything, reads, poles, skip_gain[None], doc_edges, me)
    return deinterleave(mixed)


def rounded_sum(activations, weights, pieces):
    block_width = activations.shape[1] // pieces
    summed = jnp.zeros((activations.shape[0], weights.shape[1]), jnp.float32)
    for number in range(pieces):
        lower = number * block_width
        partial_value = jnp.dot(
            activations[:, lower : lower + block_width],
            weights[lower : lower + block_width],
            preferred_element_type=jnp.float32,
        ).astype(jnp.bfloat16)
        summed = summed + lax.optimization_barrier(partial_value).astype(jnp.float32)
    return summed


def local(
    mix_input,
    stream,
    doc_ids,
    log_dt,
    decay_rate,
    frequency,
    input_real,
    input_imag,
    output_real,
    output_imag,
    skip_gain,
    log_keep,
    proj_weight,
    norm_gain,
    gate_weight,
    up_weight,
    down_weight,
):
    mixed = mixing(
        mix_input, doc_ids, log_dt, decay_rate, frequency, input_real, input_imag,
        output_real, output_imag, skip_gain, log_keep,
    )
    tp_size = lax.axis_size("tp")
    spread = lax.all_to_all(mixed, "tp", split_axis=0, concat_axis=1, tiled=True)
    proj_whole = lax.all_gather(proj_weight, "tp", axis=0, tiled=True)
    branch = rounded_sum(spread, proj_whole, tp_size)
    resid = stream.astype(jnp.float32) + branch
    scale = lax.rsqrt(jnp.mean(resid * resid, axis=-1, keepdims=True) + 1e-06)
    normed = (resid * scale * norm_gain).astype(jnp.bfloat16)
    rows_all = lax.all_gather(normed, "tp", axis=0, tiled=True)
    gate = jnp.dot(
        rows_all,
        lax.all_gather(gate_weight, "sp", axis=0, tiled=True),
        preferred_element_type=jnp.float32,
    )
    upward = jnp.dot(
        rows_all,
        lax.all_gather(up_weight, "sp", axis=0, tiled=True),
        preferred_element_type=jnp.float32,
    )
    hidden = (jax.nn.silu(gate) * upward).astype(jnp.bfloat16)
    partial_out = jnp.dot(
        hidden,
        lax.all_gather(down_weight, "sp", axis=1, tiled=True),
        preferred_element_type=jnp.float32,
    )
    ffn = lax.psum_scatter(
        partial_out.astype(jnp.bfloat16), "tp", scatter_dimension=0, tiled=True
    ).astype(jnp.float32)
    return (resid + 0.5 * ffn).astype(jnp.bfloat16)


def solution(mesh):
    placed = (
        P("sp", "tp"),
        P(("sp", "tp"), None),
        P("sp"),
        P("tp"),
        P("tp", None),
        P("tp", None),
        P(None, "tp", None, None),
        P(None, "tp", None, None),
        P(None, "tp", None, None),
        P(None, "tp", None, None),
        P("tp"),
        P("tp", "sp"),
        P("tp", None),
        P(),
        P("sp", "tp"),
        P("sp", "tp"),
        P("tp", "sp"),
    )
    return jax.shard_map(
        local, mesh=mesh, in_specs=placed, out_specs=P(("sp", "tp"), None), check_vma=False
    )
```

time: 1140 us -> 412 us (0.36); the launches traced: 1120 us -> 411 us
  local copies, waits for them, and re-layouts: 328 us -> 1.95 us
  blocking collectives: 275 us -> 40.4 us
  other arithmetic: 112 us -> 7.02 us
  loops' own time: 39.4 us -> 0 us
  matrix products: 35.7 us -> 19.7 us
  Pallas kernels: 0 us -> 11.9 us
    all_gather x8 -> x1, blocking collectives: 247 us -> 33.1 us  [mixing(): everything = lax.all_gather(total, 'sp')]
    slice x115 -> x2, local copies, waits for them, and re-layouts: 179 us -> 0.58 us  [the longest x1 0.58 us: mixing(): doc_edges = jnp.stack([doc_ids[0], doc_ids[-1]]).astype(F32)]
    unnamed x455 -> x18, local copies, waits for them, and re-layouts: 66.1 us -> 0.04 us
    another operation x2 -> x0, loops' own time: 39.4 us -> none  [prefix(): return lax.fori_loop(0, devices, hop, start)]
    unnamed x35 -> x0, other arithmetic: 37.9 us -> none
    add x69 -> x0, other arithmetic: 35 us -> none  [the longest x32 12.6 us: blocked_scan(): outer = lax.associative_scan(pair_combine, ends, reverse=reverse, axis=0)]
    unnamed x1 -> x0, blocking collectives: 21.3 us -> none
    sub x8 -> x0, local copies, waits for them, and re-layouts: 18.7 us -> none  [the longest x4 9.38 us: blocked_scan(): local_real = inner_sr + inner_mr * carry_sr - inner_mi * carry_si]
  transfers between devices with their start and end apart: 6 -> 6, of which waited for: 5 -> 5; matrix products, arithmetic and copies ran while one was open for 40% -> 3% of each run, Pallas kernels for 0% -> 3%
where the time goes in v1:
time: 412 us; the launch traced here: 411 us
  waiting for transfers between devices  316 us (77%)
  blocking collectives  40.4 us (10%)
  matrix products  19.7 us (5%)
  between operations  13.7 us (3%)
  Pallas kernels  11.9 us (3%)
  other arithmetic  7.02 us (2%)
    all_gather x1, waiting for transfers between devices, local(): lax.all_gather(gate_weight, 'sp', axis=0, tiled=True)  94.5 us
    all_gather x1, waiting for transfers between devices, local(): lax.all_gather(down_weight, 'sp', axis=1, tiled=True)  93.2 us
    all_gather x1, waiting for transfers between devices, local(): lax.all_gather(up_weight, 'sp', axis=0, tiled=True)  87.8 us
    all_gather x1, blocking collectives, mixing(): everything = lax.all_gather(total, 'sp')  33.1 us
    reduce_scatter x1, waiting for transfers between devices, local(): lax.psum_scatter(partial_out.astype(jnp.bfloat16), 'tp', scatter_dimensio...  23.1 us
    all_gather x1, waiting for transfers between devices, local(): rows_all = lax.all_gather(normed, 'tp', axis=0, tiled=True)  14.9 us
    dot_general x1, matrix products, local(): jnp.dot(hidden, lax.all_gather(down_weight, 'sp', axis=1, tiled=True), pr...  8.81 us
  transfers between devices with their start and end apart: 6, of which 5 were waited for; matrix products, arithmetic and copies ran while one was open for 3% of the time, Pallas kernels for 3%

profile of v1, /device:TPU:0, one launch (start us, length us, event | category | flops | bytes accessed | tf_op | source)
XLA Modules:
  0.0 411.1 jit_solution(7177683196192668571)
XLA Ops:
  6.5 0.0 copy-start.6
  6.5 0.0 copy-start.5
  6.5 0.0 copy-start.4
  6.5 0.0 copy-start.1
  6.5 0.0 copy-start.2
  6.5 0.0 all-gather.7.cloned.1.call-start
  6.6 0.7 all-gather.7.cloned.1.call-update
  7.3 0.0 all-gather.9.cloned.1.call-start
  7.3 0.7 exponential_negate_fusion
  8.0 0.8 cosine_multiply_fusion
  8.8 1.1 subtract_bitcast_fusion
  10.0 0.6 copy.50
  10.6 0.0 copy-start
  10.6 0.1 stack_reshape.14
  10.7 0.1 stack_reshape.15
  10.8 0.0 copy-done.6
  10.8 0.1 compare_convert_fusion
  10.9 0.1 pad_maximum_fusion.5
  10.9 0.0 copy-done.5
  11.0 0.1 reshape_squeeze.6
  11.1 0.1 copy.48
  11.2 0.1 reshape_squeeze.7
  11.3 0.1 copy.49
  11.4 0.0 copy-done.4
  11.4 0.1 copy.56
  11.5 0.0 copy-done.1
  11.5 0.0 copy-done.2
  11.7 0.6 fusion.12
  12.2 1.3 add_convert_fusion.1.doc_ref
  13.6 5.4 %drive.1 = (f32[4,256,1024]{2,1,0:T(8,128)S(1)}, f32[2,4,8,1024]{3,2,1,0:T(8,128)S(1)}, f32[16,1024]{1,0:T(8,128)S(1)}) custom-call(bf16[256,256]{1,0:T(8,128)(2,1)S(1)} %bitcast.45, f32[2,256,16]{2,1,0:T(8,128)S(1)} %pad_maximum_fusion.2.keep_ref, f32[4,1024,16]{2,1,0:T(8,128)S(1)} %bitcast.42, f32[2,1024]{1,0:T(2,128)S(1)} %pad_maximum_fusion.3.pole_ref, ...), custom_call_target="tpu_custom_call" | custom-call | flops 100000000 | bytes 6291456 | tf_op jit(solution)/shard_map/drive/pallas_call | solution.py:261
  18.9 33.1 %all-gather = f32[128,1024]{1,0:T(8,128)S(1)} all-gather(f32[16,1024]{1,0:T(8,128)S(1)} %get-tuple-element.10), channel_id=2, replica_groups=mesh['sp'=8,'tp'=4] {'sp'}, dimensions={0}, use_global_device_ids=true | all-gather | bytes 589824 | tf_op jit(solution)/shard_map/all_gather | solution.py:275
  52.0 0.0 copy-done
  52.0 6.5 %read.1 = bf16[256,256]{1,0:T(8,128)(2,1)S(1)} custom-call(bf16[256,256]{1,0:T(8,128)(2,1)S(1)} %bitcast.46, f32[2,256,16]{2,1,0:T(8,128)S(1)} %pad_maximum_fusion.2.keep_ref, f32[4,256,1024]{2,1,0:T(8,128)S(1)} %get-tuple-element.8.drive_ref, f32[2,4,8,1024]{3,2,1,0:T(8,128)S(1)} %get-tuple-element.9.chunk_ref, f32[8,16,1024]{2,1,0:T(8,128)S(1)} %bitcast.44, ...), custom_call_target="tpu_custom_call" | custom-call | flops 100000000 | bytes 6291456 | tf_op jit(solution)/shard_map/read/pallas_call | solution.py:278
  58.6 0.0 copy-start.3
  58.6 0.0 copy-start.7
  58.6 7.3 %all_to_all.19 = bf16[4,64,256]{2,1,0:T(8,128)(2,1)S(1)} all-to-all(bf16[4,64,256]{2,1,0:T(8,128)(2,1)S(1)} %bitcast.49), channel_id=1, replica_groups=mesh['sp'=8,'tp'=4] {'tp'}, dimensions={0} | all-to-all | bytes 262144 | tf_op jit(solution)/shard_map/all_to_all | solution.py:335
  65.9 0.0 all-gather.7.cloned.1.call-done
  65.9 1.5 convolution_convert_fusion.4
  67.5 1.5 convolution_convert_fusion.3
  69.0 1.5 convolution_convert_fusion.2
  70.5 1.5 convolution_convert_fusion.1
  72.1 0.0 copy-done.3
  72.1 0.3 multiply_reduce_fusion
  72.4 0.0 copy-done.7
  72.4 0.8 multiply_convert_fusion
  73.2 0.0 all-gather.9.cloned.1.call-update
  73.2 0.0 all-gather.11.cloned.1.call-start
  73.3 0.7 all-gather.11.cloned.1.call-update
  74.0 0.0 all-gather.13.cloned.1.call-start
  74.0 0.5 all-gather.13.cloned.1.call-update
  74.6 0.0 all-gather.15.cloned.1.call-start
  74.6 0.5 all-gather.15.cloned.1.call-update
  75.1 0.2 reduce-scatter.2.cloned.1.call-start
  75.4 14.9 %all-gather.9.cloned.1.call-done = bf16[256,2048]{1,0:T(8,128)(2,1)} async-done(((bf16[64,2048]{1,0:T(8,128)(2,1)}), bf16[256,2048]{1,0:T(8,128)(2,1)}) %all-gather.9.cloned.1.call-update) | async-done | bytes 1048592 | tf_op jit(solution)/shard_map/all_gather | solution.py:341
  90.3 0.0 copy-start.8
  90.3 94.5 %all-gather.11.cloned.1.call-done = bf16[2048,1408]{1,0:T(8,128)(2,1)} async-done(((bf16[256,1408]{1,0:T(8,128)(2,1)}), bf16[2048,1408]{1,0:T(8,128)(2,1)}) %all-gather.11.cloned.1.call-update) | async-done | bytes 5767184 | tf_op jit(solution)/shard_map/all_gather | solution.py:344
  184.8 4.8 %fusion.13 = f32[256,1408]{1,0:T(8,128)S(1)} fusion(bf16[256,2048]{1,0:T(8,128)(2,1)} %all-gather.9.cloned.1.call-done, bf16[2048,1408]{1,0:T(8,128)(2,1)} %all-gather.11.cloned.1.call-done), kind=kOutput, calls=%fused_computation.45 | convolution fusion | flops 1476395008 | bytes 8257536 | tf_op jit(solution)/shard_map/dot_general | solution.py:342
  189.6 87.8 %all-gather.13.cloned.1.call-done = bf16[2048,1408]{1,0:T(8,128)(2,1)} async-done(((bf16[256,1408]{1,0:T(8,128)(2,1)}), bf16[2048,1408]{1,0:T(8,128)(2,1)}) %all-gather.13.cloned.1.call-update) | async-done | bytes 5767184 | tf_op jit(solution)/shard_map/all_gather | solution.py:349
  277.4 93.2 %all-gather.15.cloned.1.call-done = bf16[1408,2048]{1,0:T(8,128)(2,1)} async-done(((bf16[1408,256]{1,0:T(8,128)(2,1)}), bf16[1408,2048]{1,0:T(8,128)(2,1)}) %all-gather.15.cloned.1.call-update) | async-done | bytes 5767184 | tf_op jit(solution)/shard_map/all_gather | solution.py:355
  370.6 0.0 copy-done.8
  370.6 8.8 %convolution_convert_fusion = bf16[256,2048]{1,0:T(8,128)(2,1)} fusion(bf16[1408,2048]{1,0:T(8,128)(2,1)} %all-gather.15.cloned.1.call-done, bf16[256,2048]{1,0:T(8,128)(2,1)S(1)} %copy-done.8, bf16[2048,1408]{1,0:T(8,128)(2,1)} %all-gather.13.cloned.1.call-done, f32[256,1408]{1,0:T(8,128)S(1)} %fusion.13), kind=kOutput, calls=%fused_computation.2 | convolution fusion | flops 2955476992 | bytes 15073280 | tf_op jit(solution)/shard_map/dot_general | solution.py:353
  379.4 0.0 reduce-scatter.2.cloned.1.call-update
  379.4 23.1 %reduce-scatter.2.cloned.1.call-done = bf16[64,2048]{1,0:T(8,128)(2,1)} async-done(((bf16[256,2048]{1,0:T(8,128)(2,1)}), bf16[64,2048]{1,0:T(8,128)(2,1)}) %reduce-scatter.2.cloned.1.call-update) | async-done | bytes 262160 | tf_op jit(solution)/shard_map/reduce_scatter | solution.py:358
  402.5 1.7 add_convert_fusion
  (13 shorter events, 0.2 us)
Async XLA Ops:
  6.5 4.2 %copy-start.6 = (s32[256]{0:T(256)S(1)}, s32[256]{0:T(256)}, u32[]{:S(2)}) copy-start(s32[256]{0:T(256)} %param.19) | copy-start | bytes 3076
  6.5 4.4 %copy-start.5 = (f32[16,256]{1,0:T(8,128)S(1)}, f32[16,256]{1,0:T(8,128)}, u32[]{:S(2)}) copy-start(f32[16,256]{1,0:T(8,128)} %param.28) | copy-start | bytes 49156
  6.5 4.9 %copy-start.4 = (bf16[256,256]{1,0:T(8,128)(2,1)S(1)}, bf16[256,256]{1,0:T(8,128)(2,1)}, u32[]{:S(2)}) copy-start(bf16[256,256]{1,0:T(8,128)(2,1)} %param.17) | copy-start | bytes 393220
  6.5 5.0 %copy-start.1 = (f32[2,16,16,64]{3,2,1,0:T(8,128)S(1)}, f32[2,16,16,64]{3,2,1,0:T(8,128)}, u32[]{:S(2)}) copy-start(f32[2,16,16,64]{3,2,1,0:T(8,128)} %param.26) | copy-start | bytes 393220
  6.5 5.0 %copy-start.2 = (f32[2,16,16,64]{3,2,1,0:T(8,128)S(1)}, f32[2,16,16,64]{3,2,1,0:T(8,128)}, u32[]{:S(2)}) copy-start(f32[2,16,16,64]{3,2,1,0:T(8,128)} %param.25) | copy-start | bytes 393220
  6.5 59.4 %all-gather.7.cloned.1.call-start = ((), (), s32[]{:S(2)}) async-start(), calls=%async_computation.2 | async-start | bytes 5242880 | tf_op jit(solution)/shard_map/all_gather | solution.py:336
  7.3 83.0 %all-gather.9.cloned.1.call-start = ((), (), s32[]{:S(2)}) async-start(), calls=%async_computation.3 | async-start | bytes 1310720 | tf_op jit(solution)/shard_map/all_gather | solution.py:341
  10.6 41.4 %copy-start = (f32[256]{0:T(256)S(1)}, f32[256]{0:T(256)}, u32[]{:S(2)}) copy-start(f32[256]{0:T(256)} %param.27) | copy-start | bytes 3076
  58.6 13.5 %copy-start.3 = (bf16[64,2048]{1,0:T(8,128)(2,1)S(1)}, bf16[64,2048]{1,0:T(8,128)(2,1)}, u32[]{:S(2)}) copy-start(bf16[64,2048]{1,0:T(8,128)(2,1)} %param.18) | copy-start | bytes 786436
  58.6 13.8 %copy-start.7 = (f32[2048]{0:T(1024)S(1)}, f32[2048]{0:T(1024)}, u32[]{:S(2)}) copy-start(f32[2048]{0:T(1024)} %param.30) | copy-start | bytes 24580
  73.2 111.5 %all-gather.11.cloned.1.call-start = ((), (), s32[]{:S(2)}) async-start(), calls=%async_computation.4 | async-start | bytes 6488064 | tf_op jit(solution)/shard_map/all_gather | solution.py:344
  74.0 203.4 %all-gather.13.cloned.1.call-start = ((), (), s32[]{:S(2)}) async-start(), calls=%async_computation.5 | async-start | bytes 6488064 | tf_op jit(solution)/shard_map/all_gather | solution.py:349
  74.6 296.0 %all-gather.15.cloned.1.call-start = ((), (), s32[]{:S(2)}) async-start(), calls=%async_computation.6 | async-start | bytes 6488064 | tf_op jit(solution)/shard_map/all_gather | solution.py:355
  75.1 327.4 %reduce-scatter.2.cloned.1.call-start = ((), (), s32[]{:S(2)}) async-start(), calls=%async_computation.7 | async-start | bytes 1310720 | tf_op jit(solution)/shard_map/reduce_scatter | solution.py:358
  90.3 280.3 %copy-start.8 = (bf16[256,2048]{1,0:T(8,128)(2,1)S(1)}, bf16[256,2048]{1,0:T(8,128)(2,1)}, u32[]{:S(2)}) copy-start(bf16[256,2048]{1,0:T(8,128)(2,1)} %all-gather.9.cloned.1.call-done) | copy-start | bytes 3145732
Sparse Core Ops, SparseCore 0:
  8.9 37.1 all-gather.6
  73.4 16.8 all-gather.8
  92.4 92.3 all-gather.10
  186.8 90.4 all-gather.12
  279.2 91.2 all-gather.14
  379.5 22.9 reduce-scatter.1
